TPU v7x, 256 devices: a whole 4x4x8 slice. The times are simulated.
256 devices in a mesh: rep: 2 (over z_hi), fs: 16 (over z_lo, x), tp: 8 (over y, core).
Axes of the slice: x: 4, y: 4, z: 8 (z_hi: 2, z_lo: 4; z = z_hi * 4 + z_lo), core: 2. Of those that a mesh axis runs over, the one named last changes fastest.
Arguments:
- tokens: bfloat16 [24576, 2048], P(('rep', 'fs'), 'tp'), parts along dimension 0, may hold values from -6 to 6
- mixer_gain: float32 [2048], replicated, may hold values from 0.1 to 1.9
- rec_weight: bfloat16 [2048, 2048], P('fs', 'tp'), may hold values from -0.125 to 0.125
- gate_weight: bfloat16 [2048, 2048], P('fs', 'tp'), may hold values from -0.125 to 0.125
- conv_taps: bfloat16 [4, 2048], P(None, 'tp'), may hold values from -3 to 3
- recur_map: bfloat16 [8, 256, 256], P('tp'), may hold values from -0.375 to 0.375
- input_map: bfloat16 [8, 256, 256], P('tp'), may hold values from -0.375 to 0.375
- decay_param: float32 [2048], P('tp'), may hold values from 3 to 11
- out_weight: bfloat16 [2048, 2048], P('tp', 'fs'), may hold values from -0.5 to 0.5
- mlp_gain: float32 [2048], replicated, may hold values from 0.1 to 1.9
- up_weight: bfloat16 [2048, 8192], P('fs', 'tp'), may hold values from -0.125 to 0.125
- down_weight: bfloat16 [8192, 2048], P('tp', 'fs'), may hold values from -0.0625 to 0.0625
Outputs:
- layer_out: bfloat16 [24576, 2048], P(('rep', 'fs'), 'tp'), parts along dimension 0
There are 2 independent parts, one for each index of `rep`. A program takes and returns all parts, laid end to end along the dimension named above; an argument that names none is the same for every part. Nothing has to cross between parts.
All inputs are finite; a program needn't handle non-finite values.
Results may differ from a plain program's by a relative error of at most 0.022.
Values may be sent and summed in bfloat16 or wider, within the bound.
A program may use at most 64 MiB of HBM per device.

v0:
```python
import jax
import jax.numpy as jnp
from jax import lax
from jax.sharding import PartitionSpec as P

NORM_EPSILON = 1e-06
GATE_SCALE = 8.0


def turned_gather(arrays, axis, dims):
    turned = [jnp.moveaxis(a, dim, 0) for a, dim in zip(arrays, dims)]
    widths = [t[0].size for t in turned]
    both = jnp.concatenate([t.reshape(-1, w) for t, w in zip(turned, widths)], axis=1)
    filled = lax.all_gather(both, axis, axis=0, tiled=True)
    blocks = jnp.split(filled, [sum(widths[:k]) for k in range(1, len(widths))], axis=1)
    return tuple(
        (
            jnp.moveaxis(b.reshape(-1, *t.shape[1:]), 0, dim)
            for b, t, dim in zip(blocks, turned, dims)
        )
    )


def joined_along(blocks, dim):
    blocks = jnp.moveaxis(blocks, 0, dim)
    lengths = blocks.shape
    return blocks.reshape(*lengths[:dim], lengths[dim] * lengths[dim + 1], *lengths[dim + 2 :])


def from_everyone(array, axis):
    copies = jnp.broadcast_to(array, (lax.axis_size(axis), *array.shape))
    return lax.all_to_all(copies, axis, split_axis=0, concat_axis=0, tiled=True)


def gather_directly(array, axis, dim):
    return joined_along(from_everyone(array, axis), dim)


def side_by_side(arrays, axis, dim, along):
    ends, at = ([], 0)
    for a in arrays[:-1]:
        at += a.shape[along]
        ends.append(at)
    both = jnp.concatenate(arrays, axis=along)
    return tuple(jnp.split(lax.all_gather(both, axis, axis=dim, tiled=True), ends, axis=along))


def cut_along(array, dim, count):
    lengths = array.shape
    blocks = array.reshape(*lengths[:dim], count, lengths[dim] // count, *lengths[dim + 1 :])
    return jnp.moveaxis(blocks, dim, 0)


def sent_and_summed(array, axis, dim):
    blocks = cut_along(array, dim, lax.axis_size(axis))
    arrived = lax.all_to_all(blocks, axis, split_axis=0, concat_axis=0, tiled=True)
    return arrived.astype(jnp.float32).sum(axis=0)


def rms_rows(full_rows, gain):
    widened = full_rows.astype(jnp.float32)
    inverse = lax.rsqrt(jnp.mean(widened * widened, axis=-1, keepdims=True) + NORM_EPSILON)
    return (widened * inverse * gain).astype(jnp.bfloat16)


def causal_taps(branch, conv_taps):
    widened = branch.astype(jnp.float32)
    tap_values = conv_taps.astype(jnp.float32)
    tap_count = tap_values.shape[0]
    length = widened.shape[0]
    padded = jnp.pad(widened, ((tap_count - 1, 0), (0, 0)))
    running = jnp.zeros_like(widened)
    for offset in range(tap_count):
        running = running + padded[offset : offset + length, :] * tap_values[offset]
    return running.astype(jnp.bfloat16)


def combine(earlier, latter):
    return (earlier[0] * latter[0], latter[0] * earlier[1] + latter[1])


def add_rows(operand, column_piece):
    return jnp.dot(operand, column_piece, preferred_element_type=jnp.float32)


def feature_term(whole_weight, hidden):
    return lax.dot_general(
        whole_weight, hidden, (((0,), (1,)), ((), ())), preferred_element_type=jnp.float32
    )


def recurrence(branch, gate_branch, conv_taps, recur_map, input_map, decay_param):
    length = branch.shape[0]
    block_w = recur_map.shape[1]
    conv_out = causal_taps(branch, conv_taps)
    blocks = conv_out.reshape(length, -1, block_w)
    recur_gate = jax.nn.sigmoid(
        jnp.einsum("lnc,ncd->lnd", blocks, recur_map, preferred_element_type=jnp.float32).reshape(
            length, -1
        )
    )
    input_gate = jax.nn.sigmoid(
        jnp.einsum("lnc,ncd->lnd", blocks, input_map, preferred_element_type=jnp.float32).reshape(
            length, -1
        )
    )
    log_decay = -GATE_SCALE * recur_gate * jax.nn.softplus(-decay_param)
    decay_rate = jnp.exp(log_decay)
    drive_term = jnp.sqrt(-jnp.expm1(2.0 * log_decay)) * (input_gate * conv_out.astype(jnp.float32))
    _, states = lax.associative_scan(combine, (decay_rate, drive_term), axis=0)
    return (states * jax.nn.gelu(gate_branch.astype(jnp.float32))).astype(jnp.bfloat16)


def shards(
    tokens,
    mixer_gain,
    rec_weight,
    gate_weight,
    conv_taps,
    recur_map,
    input_map,
    decay_param,
    out_weight,
    mlp_gain,
    up_weight,
    down_weight,
):
    up_whole, down_whole = turned_gather((up_weight, down_weight), "fs", (0, 1))
    full_rows = gather_directly(tokens, "tp", 1)
    normed = rms_rows(full_rows, mixer_gain)
    pieces = side_by_side((rec_weight, gate_weight), "fs", 0, 1)
    branch_sum = add_rows(normed, pieces[0])
    gate_sum = add_rows(normed, pieces[1])
    branch = branch_sum.astype(jnp.bfloat16)
    gate_branch = gate_sum.astype(jnp.bfloat16)
    mixed_out = recurrence(branch, gate_branch, conv_taps, recur_map, input_map, decay_param)
    out_whole = gather_directly(out_weight, "fs", 1)
    mixer_out = sent_and_summed(feature_term(out_whole, mixed_out).astype(jnp.bfloat16), "tp", 0).T
    middle = (tokens.astype(jnp.float32) + mixer_out).astype(jnp.bfloat16)
    middle_rows = gather_directly(middle, "tp", 1)
    normed_mlp = rms_rows(middle_rows, mlp_gain)
    lifted = jnp.dot(normed_mlp, up_whole, preferred_element_type=jnp.float32)
    squared = jnp.square(jax.nn.relu(lifted)).astype(jnp.bfloat16)
    mlp_out = sent_and_summed(feature_term(down_whole, squared).astype(jnp.bfloat16), "tp", 0).T
    return (middle.astype(jnp.float32) + mlp_out).astype(jnp.bfloat16)


def solution(mesh):
    placed = (
        P(("rep", "fs"), "tp"),
        P(),
        P("fs", "tp"),
        P("fs", "tp"),
        P(None, "tp"),
        P("tp", None, None),
        P("tp", None, None),
        P("tp"),
        P("tp", "fs"),
        P(),
        P("fs", "tp"),
        P("tp", "fs"),
    )
    return jax.shard_map(
        shards, mesh=mesh, in_specs=placed, out_specs=P(("rep", "fs"), "tp"), check_vma=False
    )
```

profile of v0, /device:TPU:6, one launch (start us, length us, event | category | flops | bytes accessed | tf_op | source)
XLA Modules:
  0.0 285.1 jit_solution(8443693442468253675)
XLA Ops:
  6.5 1.6 pad_maximum_fusion.3
  8.1 1.2 copy.24
  9.3 1.9 broadcast_in_dim.6
  11.2 4.6 %all-to-all-start = ((bf16[8,768,256]{1,2,0:T(8,128)(2,1)}), bf16[8,768,256]{1,2,0:T(8,128)(2,1)S(1)}, u32[]{:S(2)}, u32[]{:S(2)}) async-start(bf16[8,768,256]{1,2,0:T(8,128)(2,1)} %broadcast_in_dim.6), calls=%async_computation | async-start | bytes 6291456 | tf_op jit(solution)/shard_map/all_to_all | solution.py:32
  15.9 1.1 copy.27
  17.0 1.8 pad_maximum_fusion
  18.8 0.9 copy.25
  19.8 34.4 %all-to-all-done = bf16[8,768,256]{1,2,0:T(8,128)(2,1)S(1)} async-done(((bf16[8,768,256]{1,2,0:T(8,128)(2,1)}), bf16[8,768,256]{1,2,0:T(8,128)(2,1)S(1)}, u32[]{:S(2)}, u32[]{:S(2)}) %all-to-all-start) | async-done | bytes 3145760 | tf_op jit(solution)/shard_map/all_to_all | solution.py:32
  54.2 1.1 broadcast_in_dim.7
  55.3 8.9 %all-to-all-start.1 = ((bf16[16,256,128]{1,2,0:T(8,128)(2,1)}), bf16[16,256,128]{1,2,0:T(8,128)(2,1)}, u32[]{:S(2)}, u32[]{:S(2)}) async-start(bf16[16,256,128]{1,2,0:T(8,128)(2,1)} %broadcast_in_dim.7), calls=%async_computation.1 | async-start | bytes 2097152 | tf_op jit(solution)/shard_map/all_to_all | solution.py:32
  64.2 0.7 multiply_reduce_fusion.1
  64.9 2.5 fusion.3
  67.4 25.0 %all-gather.3.cloned.1.call-done = bf16[2048,512]{1,0:T(8,128)(2,1)} async-done(((bf16[128,512]{1,0:T(8,128)(2,1)}), bf16[2048,512]{1,0:T(8,128)(2,1)}) %all-gather.3.cloned.1.call-update) | async-done | bytes 2097168 | tf_op jit(solution)/shard_map/all_gather | solution.py:45
  92.4 3.2 %fusion.22 = f32[768,256]{1,0:T(8,128)S(1)} fusion(bf16[768,2048]{0,1:T(8,128)(2,1)} %fusion.3, bf16[2048,512]{1,0:T(8,128)(2,1)} %all-gather.3.cloned.1.call-done), kind=kOutput, calls=%fused_computation.35 | convolution fusion | flops 805699584 | bytes 4980736 | tf_op jit(solution)/shard_map/dot_general | solution.py:83
  95.6 0.4 add_convert_fusion
  95.9 0.5 fusion.74
  96.5 0.7 fusion.17
  97.2 0.5 slice.245
  97.7 0.5 slice.246
  98.2 1.5 slice.244
  99.6 1.4 slice.248
  101.1 1.2 fusion.65
  102.3 0.1 slice.251
  102.4 0.1 slice.252
  102.6 0.1 slice.250
  102.7 0.7 slice.254
  103.5 1.0 fusion.66
  105.4 0.6 fusion.55
  106.0 0.6 slice.320
  106.6 0.6 slice.302
  107.2 0.6 slice.319
  107.8 0.6 slice.304
  108.5 0.6 slice.318
  109.1 0.7 slice.255
  109.7 0.7 slice.306
  110.4 0.3 slice.308
  110.7 0.9 slice.249
  111.6 0.5 slice.310
  112.1 0.5 slice.243
  112.6 0.7 pad_maximum_fusion.7
  113.4 0.7 fusion.54
  114.1 0.7 pad_maximum_fusion.6
  114.8 0.8 fusion.53
  115.7 0.7 pad_maximum_fusion.5
  116.9 1.9 pad.77
  118.8 0.1 fusion.44
  118.9 1.9 pad.76
  120.8 6.4 %convolution_convert_fusion = bf16[768,2048]{1,0:T(8,128)(2,1)S(1)} fusion(bf16[256,2048]{0,1:T(8,128)(2,1)} %bitcast.9, bf16[768,2048]{0,1:T(8,128)(2,1)} %fusion.3, bf16[2048,512]{1,0:T(8,128)(2,1)} %all-gather.3.cloned.1.call-done, f32[768,256]{1,0:T(8,128)} %pad.76, f32[768,256]{1,0:T(8,128)} %pad.77), kind=kOutput, calls=%fused_computation.15 | convolution fusion | flops 1614741504 | bytes 9961472 | tf_op jit(solution)/shard_map/dot_general | solution.py:87
  127.2 0.2 copy.32
  127.5 42.6 %all_to_all.25 = bf16[8,256,768]{1,2,0:T(8,128)(2,1)S(1)} all-to-all(bf16[8,256,768]{1,2,0:T(8,128)(2,1)S(1)} %bitcast.57), channel_id=1, replica_groups=mesh['rep'=2,'fs'=16,'tp'=8] {'tp'}, dimensions={0} | all-to-all | bytes 6291456 | tf_op jit(solution)/shard_map/all_to_all | solution.py:56
  170.1 0.4 convert_reduce_fusion.1
  170.5 0.6 copy-done.3
  171.1 0.1 fusion.41
  171.2 0.2 copy.28
  171.3 0.2 broadcast_in_dim.16
  171.6 40.9 %all_to_all.26 = bf16[8,768,256]{1,2,0:T(8,128)(2,1)S(1)} all-to-all(bf16[8,768,256]{1,2,0:T(8,128)(2,1)S(1)} %broadcast_in_dim.16), channel_id=1, replica_groups=mesh['rep'=2,'fs'=16,'tp'=8] {'tp'}, dimensions={0} | all-to-all | bytes 6291456 | tf_op jit(solution)/shard_map/all_to_all | solution.py:32
  212.5 0.7 multiply_reduce_fusion
  213.2 2.5 fusion.1
  215.7 5.9 %all-gather.5.cloned.1.call-done = bf16[2048,2048]{0,1:T(8,128)(2,1)} async-done(((bf16[128,2048]{0,1:T(8,128)(2,1)}), bf16[2048,2048]{0,1:T(8,128)(2,1)}) %all-gather.5.cloned.1.call-update) | async-done | bytes 8388624 | tf_op jit(solution)/shard_map/all_gather | solution.py:14
  221.6 12.9 %fusion.8 = bf16[2048,768]{1,0:T(8,128)(2,1)} fusion(bf16[2048,2048]{0,1:T(8,128)(2,1)} %all-gather.5.cloned.1.call-done, bf16[768,2048]{0,1:T(8,128)(2,1)} %fusion.1), kind=kOutput, calls=%fused_computation.14 | convolution fusion | flops 6446383104 | bytes 14680064 | tf_op jit(solution)/shard_map/dot_general | solution.py:87
  234.5 42.1 %all_to_all.27 = bf16[8,256,768]{2,1,0:T(8,128)(2,1)S(1)} all-to-all(bf16[8,256,768]{2,1,0:T(8,128)(2,1)} %bitcast.59), channel_id=1, replica_groups=mesh['rep'=2,'fs'=16,'tp'=8] {'tp'}, dimensions={0} | all-to-all | bytes 6291456 | tf_op jit(solution)/shard_map/all_to_all | solution.py:56
  276.7 0.4 convert_reduce_fusion
  277.1 0.3 copy.29
  277.4 0.8 fusion.40
  (110 shorter events, 1.5 us)
Async XLA Ops:
  6.5 89.4 %copy-start = (bf16[1,256,256]{2,1,0:T(8,128)(2,1)S(1)}, bf16[1,256,256]{2,1,0:T(8,128)(2,1)}, u32[]{:S(2)}) copy-start(bf16[1,256,256]{2,1,0:T(8,128)(2,1)} %param.17) | copy-start | bytes 393220
  6.5 85.8 %all-gather.3.cloned.1.call-start = ((), (), s32[]{:S(2)}) async-start(), calls=%async_computation.5 | async-start | bytes 2228224 | tf_op jit(solution)/shard_map/all_gather | solution.py:45
  11.2 7.6 %copy-start.10 = (f32[256]{0:T(256)S(1)}, f32[256]{0:T(256)}, u32[]{:S(2)}) copy-start(f32[256]{0:T(256)} %param.19) | copy-start | bytes 3076
  11.2 8.6 %copy-start.9 = (bf16[4,256]{1,0:T(4,128)(2,1)S(1)}, bf16[4,256]{1,0:T(4,128)(2,1)}, u32[]{:S(2)}) copy-start(bf16[4,256]{1,0:T(4,128)(2,1)} %param.16) | copy-start | bytes 6148
  11.2 43.0 %all-to-all-start = ((bf16[8,768,256]{1,2,0:T(8,128)(2,1)}), bf16[8,768,256]{1,2,0:T(8,128)(2,1)S(1)}, u32[]{:S(2)}, u32[]{:S(2)}) async-start(bf16[8,768,256]{1,2,0:T(8,128)(2,1)} %broadcast_in_dim.6), calls=%async_computation | async-start | bytes 6291456 | tf_op jit(solution)/shard_map/all_to_all | solution.py:32
  15.8 205.8 %all-gather.5.cloned.1.call-start = ((), (), s32[]{:S(2)}) async-start(), calls=%async_computation.6 | async-start | bytes 8912896 | tf_op jit(solution)/shard_map/all_gather | solution.py:14
  19.8 45.1 %copy-start.7 = (f32[2048]{0:T(1024)S(1)}, f32[2048]{0:T(1024)}, u32[]{:S(2)}) copy-start(f32[2048]{0:T(1024)} %param.13) | copy-start | bytes 24580
  55.3 65.5 %all-to-all-start.1 = ((bf16[16,256,128]{1,2,0:T(8,128)(2,1)}), bf16[16,256,128]{1,2,0:T(8,128)(2,1)}, u32[]{:S(2)}, u32[]{:S(2)}) async-start(bf16[16,256,128]{1,2,0:T(8,128)(2,1)} %broadcast_in_dim.7), calls=%async_computation.1 | async-start | bytes 2097152 | tf_op jit(solution)/shard_map/all_to_all | solution.py:32
  95.5 0.9 copy-start.11
  97.2 15.4 %copy-start.2 = (f32[768,256]{1,0:T(8,128)}, f32[768,256]{1,0:T(8,128)S(1)}, u32[]{:S(2)}) copy-start(f32[768,256]{1,0:T(8,128)S(1)} %fusion.17) | copy-start | bytes 2359300
  111.6 4.9 %copy-start.5 = (f32[95,256]{1,0:T(8,128)S(1)}, f32[95,256]{1,0:T(8,128)}, u32[]{:S(2)}) copy-start(f32[95,256]{1,0:T(8,128)} %slice.255) | copy-start | bytes 291844
  111.6 4.9 %copy-start.6 = (f32[95,256]{1,0:T(8,128)S(1)}, f32[95,256]{1,0:T(8,128)}, u32[]{:S(2)}) copy-start(f32[95,256]{1,0:T(8,128)} %slice.306) | copy-start | bytes 291844
  111.6 5.0 %copy-start.4 = (f32[191,256]{1,0:T(8,128)S(1)}, f32[191,256]{1,0:T(8,128)}, u32[]{:S(2)}) copy-start(f32[191,256]{1,0:T(8,128)} %slice.249) | copy-start | bytes 586756
  116.7 2.2 slice-start
  170.1 1.0 copy-start.3
  212.5 0.7 copy-start.8
  234.5 43.7 %copy-start.1 = (bf16[1,256,256]{2,1,0:T(8,128)(2,1)S(1)}, bf16[1,256,256]{2,1,0:T(8,128)(2,1)}, u32[]{:S(2)}) copy-start(bf16[1,256,256]{2,1,0:T(8,128)(2,1)} %param.17) | copy-start | bytes 393220
Sparse Core Ops, SparseCore 0:
  9.1 83.1 all-gather.2
  94.1 127.4 all-gather.4
where the time goes:
time: 286 us; the launch traced here: 285 us
  blocking collectives  126 us (44%)
  waiting for transfers between devices  65.4 us (23%)
  local copies, waits for them, and re-layouts  23.9 us (8%)
  matrix products  23.7 us (8%)
  other arithmetic  18.9 us (7%)
  between operations  14 us (5%)
  starting transfers between devices  13.5 us (5%)
    all_to_all x2, blocking collectives, sent_and_summed(): lax.all_to_all(blocks, axis, split_axis=0, concat_axis=0, tiled=True)  84.7 us
    all_to_all x1, blocking collectives, from_everyone(): return lax.all_to_all(copies, axis, split_axis=0, concat_axis=0, tiled=True)  40.9 us
    all_to_all x2, waiting for transfers between devices, from_everyone(): return lax.all_to_all(copies, axis, split_axis=0, concat_axis=0, tiled=True)  34.4 us
    all_gather x1, waiting for transfers between devices, side_by_side(): lax.all_gather(both, axis, axis=dim, tiled=True)  25 us
    dot_general x2, matrix products, feature_term(): lax.dot_general(whole_weight, hidden, (((0,), (1,)), ((), ())), preferred...  19.3 us
    all_to_all x2, starting transfers between devices, from_everyone(): return lax.all_to_all(copies, axis, split_axis=0, concat_axis=0, tiled=True)  13.5 us
    slice x57, local copies, waits for them, and re-layouts, recurrence(): _, states = lax.associative_scan(combine, (decay_rate, drive_term), axis=0)  12.1 us
    all_gather x1, waiting for transfers between devices, turned_gather(): filled = lax.all_gather(both, axis, axis=0, tiled=True)  5.94 us
  transfers between devices with their start and end apart: 4, of which 3 were waited for; matrix products, arithmetic and copies ran while one was open for 17% of the time, Pallas kernels for 0%

commit v1 on v0

--- a/solution.py
+++ b/solution.py
@@ -11,7 +11,9 @@
     turned = [jnp.moveaxis(a, dim, 0) for a, dim in zip(arrays, dims)]
     widths = [t[0].size for t in turned]
     both = jnp.concatenate([t.reshape(-1, w) for t, w in zip(turned, widths)], axis=1)
-    filled = lax.all_gather(both, axis, axis=0, tiled=True)
+    filled = jnp.concatenate(
+        lax.all_to_all(jnp.stack([both] * lax.axis_size(axis)), axis, 0, 0), axis=0
+    )
     blocks = jnp.split(filled, [sum(widths[:k]) for k in range(1, len(widths))], axis=1)
     return tuple(
         (

time: 286 us -> 474 us (1.66)
  the two profiles are of different devices: /device:TPU:6 before, /device:TPU:64 now
where the time goes in v1:
time: 474 us; the launch traced here: 473 us
  waiting for transfers between devices  275 us (58%)
  blocking collectives  84.2 us (18%)
  local copies, waits for them, and re-layouts  30.8 us (6%)
  starting transfers between devices  28.9 us (6%)
  matrix products  24 us (5%)
  other arithmetic  15.8 us (3%)
  between operations  14.2 us (3%)
    all_to_all x1, waiting for transfers between devices, turned_gather(): lax.all_to_all(jnp.stack([both] * lax.axis_size(axis)), axis, 0, 0)  180 us
    all_to_all x2, blocking collectives, sent_and_summed(): lax.all_to_all(blocks, axis, split_axis=0, concat_axis=0, tiled=True)  84.2 us
    all_to_all x3, waiting for transfers between devices, from_everyone(): return lax.all_to_all(copies, axis, split_axis=0, concat_axis=0, tiled=True)  71.5 us
    all_gather x1, waiting for transfers between devices, side_by_side(): lax.all_gather(both, axis, axis=dim, tiled=True)  23.3 us
    dot_general x2, matrix products, feature_term(): lax.dot_general(whole_weight, hidden, (((0,), (1,)), ((), ())), preferred...  17.5 us
    all_to_all x3, starting transfers between devices, from_everyone(): return lax.all_to_all(copies, axis, split_axis=0, concat_axis=0, tiled=True)  16.3 us
    all_to_all x1, starting transfers between devices, turned_gather(): lax.all_to_all(jnp.stack([both] * lax.axis_size(axis)), axis, 0, 0)  12.6 us
    slice x57, local copies, waits for them, and re-layouts, recurrence(): _, states = lax.associative_scan(combine, (decay_rate, drive_term), axis=0)  10.3 us
  transfers between devices with their start and end apart: 5, of which 4 were waited for; matrix products, arithmetic and copies ran while one was open for 9% of the time, Pallas kernels for 0%

profile of v1, /device:TPU:64, one launch (start us, length us, event | category | flops | bytes accessed | tf_op | source)
XLA Modules:
  0.0 472.5 jit_solution(6689349311859390379)
XLA Ops:
  6.5 1.6 pad_maximum_fusion.3
  8.1 1.2 copy.27
  9.3 1.8 broadcast_in_dim.6
  11.2 4.6 all-to-all-start
  15.8 0.1 copy.28
  15.9 38.2 %all-to-all-done = bf16[8,768,256]{1,2,0:T(8,128)(2,1)S(1)} async-done(((bf16[8,768,256]{1,2,0:T(8,128)(2,1)}), bf16[8,768,256]{1,2,0:T(8,128)(2,1)S(1)}, u32[]{:S(2)}, u32[]{:S(2)}) %all-to-all-start) | async-done | bytes 3145760 | tf_op jit(solution)/shard_map/all_to_all | solution.py:34
  54.2 1.1 broadcast_in_dim.7
  55.2 8.0 %all-to-all-start.1 = ((bf16[16,256,128]{1,2,0:T(8,128)(2,1)}), bf16[16,256,128]{1,2,0:T(8,128)(2,1)}, u32[]{:S(2)}, u32[]{:S(2)}) async-start(bf16[16,256,128]{1,2,0:T(8,128)(2,1)} %broadcast_in_dim.7), calls=%async_computation.1 | async-start | bytes 2097152 | tf_op jit(solution)/shard_map/all_to_all | solution.py:34
  63.3 0.7 multiply_reduce_fusion.1
  64.0 2.4 fusion.3
  66.4 23.3 %all-gather.2.cloned.1.call-done = bf16[2048,512]{1,0:T(8,128)(2,1)} async-done(((bf16[128,512]{1,0:T(8,128)(2,1)}), bf16[2048,512]{1,0:T(8,128)(2,1)}) %all-gather.2.cloned.1.call-update) | async-done | bytes 2097168 | tf_op jit(solution)/shard_map/all_gather | solution.py:47
  89.7 3.2 fusion.22
  92.9 0.4 add_convert_fusion
  93.2 1.4 fusion.74
  94.6 0.5 slice.248
  95.1 0.5 slice.244
  95.6 1.9 fusion.17
  97.5 1.6 slice.246
  99.1 1.5 slice.245
  100.5 1.2 fusion.65
  101.7 0.1 slice.254
  101.9 0.1 slice.250
  102.0 0.1 slice.252
  102.2 0.7 slice.251
  102.9 1.0 fusion.66
  104.9 0.6 fusion.55
  105.5 0.5 slice.310
  106.0 0.5 slice.243
  106.5 1.0 slice.255
  107.5 0.8 slice.267
  108.4 0.9 slice.261
  109.3 0.3 slice.308
  109.6 0.3 slice.249
  110.0 0.7 pad_maximum_fusion.7
  111.1 0.1 pad.75
  111.2 0.1 pad.74
  111.4 0.1 fusion.44
  111.5 0.3 slice-done
  111.8 2.0 pad.76
  113.7 2.0 pad.77
  115.8 6.4 %convolution_convert_fusion = bf16[768,2048]{1,0:T(8,128)(2,1)S(1)} fusion(bf16[256,2048]{0,1:T(8,128)(2,1)} %bitcast.9, bf16[768,2048]{0,1:T(8,128)(2,1)} %fusion.3, bf16[2048,512]{1,0:T(8,128)(2,1)} %all-gather.2.cloned.1.call-done, f32[768,256]{1,0:T(8,128)} %pad.76, f32[768,256]{1,0:T(8,128)} %pad.77), kind=kOutput, calls=%fused_computation.15 | convolution fusion | flops 1614741504 | bytes 9961472 | tf_op jit(solution)/shard_map/dot_general | solution.py:89
  122.2 0.2 copy.36
  122.4 43.2 %all_to_all.30 = bf16[8,256,768]{1,2,0:T(8,128)(2,1)S(1)} all-to-all(bf16[8,256,768]{1,2,0:T(8,128)(2,1)S(1)} %bitcast.58), channel_id=1, replica_groups=mesh['rep'=2,'fs'=16,'tp'=8] {'tp'}, dimensions={0} | all-to-all | bytes 6291456 | tf_op jit(solution)/shard_map/all_to_all | solution.py:58
  165.6 0.4 convert_reduce_fusion.1
  166.0 0.5 copy-done.5
  166.6 0.1 fusion.41
  166.7 0.2 copy.32
  166.9 1.8 broadcast_in_dim.16
  168.7 3.6 all-to-all-start.4
  172.4 1.1 copy.30
  173.5 1.8 pad_maximum_fusion
  175.3 2.1 copy.31
  177.4 33.3 %all-to-all-done.4 = bf16[8,768,256]{1,2,0:T(8,128)(2,1)S(1)} async-done(((bf16[8,768,256]{1,2,0:T(8,128)(2,1)}), bf16[8,768,256]{1,2,0:T(8,128)(2,1)S(1)}, u32[]{:S(2)}, u32[]{:S(2)}) %all-to-all-start.4) | async-done | bytes 3145760 | tf_op jit(solution)/shard_map/all_to_all | solution.py:34
  210.7 5.4 %stack.2 = bf16[16,128,2048]{2,1,0:T(8,128)(2,1)} broadcast(bf16[128,2048]{1,0:T(8,128)(2,1)} %copy.31), dimensions={1,2} | broadcast | bytes 8912896 | tf_op jit(solution)/shard_map/stack | solution.py:15
  216.1 12.6 %all-to-all-start.3 = ((bf16[16,128,2048]{2,1,0:T(8,128)(2,1)}), bf16[16,128,2048]{2,1,0:T(8,128)(2,1)}, u32[]{:S(2)}, u32[]{:S(2)}) async-start(bf16[16,128,2048]{2,1,0:T(8,128)(2,1)} %stack.2), calls=%async_computation.3 | async-start | bytes 16777216 | tf_op jit(solution)/shard_map/all_to_all | solution.py:15
  228.7 0.7 multiply_reduce_fusion
  229.4 2.4 fusion.1
  231.8 179.8 %all-to-all-done.3 = bf16[16,128,2048]{2,1,0:T(8,128)(2,1)} async-done(((bf16[16,128,2048]{2,1,0:T(8,128)(2,1)}), bf16[16,128,2048]{2,1,0:T(8,128)(2,1)}, u32[]{:S(2)}, u32[]{:S(2)}) %all-to-all-start.3) | async-done | bytes 8388640 | tf_op jit(solution)/shard_map/all_to_all | solution.py:15
  411.6 11.1 %fusion.8 = bf16[2048,768]{1,0:T(8,128)(2,1)S(1)} fusion(bf16[2048,2048]{1,0:T(8,128)(2,1)} %bitcast.13, bf16[768,2048]{0,1:T(8,128)(2,1)} %fusion.1), kind=kOutput, calls=%fused_computation.14 | convolution fusion | flops 6446383104 | bytes 14680064 | tf_op jit(solution)/shard_map/dot_general | solution.py:89
  422.8 41.0 %all_to_all.31 = bf16[8,256,768]{2,1,0:T(8,128)(2,1)S(1)} all-to-all(bf16[8,256,768]{2,1,0:T(8,128)(2,1)S(1)} %bitcast.60), channel_id=1, replica_groups=mesh['rep'=2,'fs'=16,'tp'=8] {'tp'}, dimensions={0} | all-to-all | bytes 6291456 | tf_op jit(solution)/shard_map/all_to_all | solution.py:58
  463.8 0.4 convert_reduce_fusion
  464.3 0.3 copy.33
  464.5 0.3 copy-done.3
  464.8 0.8 fusion.40
  (118 shorter events, 1.4 us)
Async XLA Ops:
  6.5 86.7 %copy-start = (bf16[1,256,256]{2,1,0:T(8,128)(2,1)S(1)}, bf16[1,256,256]{2,1,0:T(8,128)(2,1)}, u32[]{:S(2)}) copy-start(bf16[1,256,256]{2,1,0:T(8,128)(2,1)} %param.17) | copy-start | bytes 393220
  6.5 83.1 %all-gather.2.cloned.1.call-start = ((), (), s32[]{:S(2)}) async-start(), calls=%async_computation.6 | async-start | bytes 2228224 | tf_op jit(solution)/shard_map/all_gather | solution.py:47
  11.1 4.6 copy-start.9
  11.2 4.7 %copy-start.13 = (f32[256]{0:T(256)S(1)}, f32[256]{0:T(256)}, u32[]{:S(2)}) copy-start(f32[256]{0:T(256)} %param.19) | copy-start | bytes 3076
  11.2 4.8 %copy-start.12 = (bf16[4,256]{1,0:T(4,128)(2,1)S(1)}, bf16[4,256]{1,0:T(4,128)(2,1)}, u32[]{:S(2)}) copy-start(bf16[4,256]{1,0:T(4,128)(2,1)} %param.16) | copy-start | bytes 6148
  11.2 43.0 %all-to-all-start = ((bf16[8,768,256]{1,2,0:T(8,128)(2,1)}), bf16[8,768,256]{1,2,0:T(8,128)(2,1)S(1)}, u32[]{:S(2)}, u32[]{:S(2)}) async-start(bf16[8,768,256]{1,2,0:T(8,128)(2,1)} %broadcast_in_dim.6), calls=%async_computation | async-start | bytes 6291456 | tf_op jit(solution)/shard_map/all_to_all | solution.py:34
  15.9 48.0 %copy-start.10 = (f32[2048]{0:T(1024)S(1)}, f32[2048]{0:T(1024)}, u32[]{:S(2)}) copy-start(f32[2048]{0:T(1024)} %param.13) | copy-start | bytes 24580
  55.2 60.5 %all-to-all-start.1 = ((bf16[16,256,128]{1,2,0:T(8,128)(2,1)}), bf16[16,256,128]{1,2,0:T(8,128)(2,1)}, u32[]{:S(2)}, u32[]{:S(2)}) async-start(bf16[16,256,128]{1,2,0:T(8,128)(2,1)} %broadcast_in_dim.7), calls=%async_computation.1 | async-start | bytes 2097152 | tf_op jit(solution)/shard_map/all_to_all | solution.py:34
  92.9 2.7 copy-start.14
  97.5 12.5 %copy-start.4 = (f32[768,256]{1,0:T(8,128)}, f32[768,256]{1,0:T(8,128)S(1)}, u32[]{:S(2)}) copy-start(f32[768,256]{1,0:T(8,128)S(1)} %fusion.17) | copy-start | bytes 2359300
  103.9 1.0 copy-start.6
  104.1 0.8 copy-start.7
  104.2 0.7 copy-start.8
  111.0 0.7 slice-start
  165.6 1.0 copy-start.5
  166.7 2.0 copy-start.2
  168.7 42.0 %all-to-all-start.4 = ((bf16[8,768,256]{1,2,0:T(8,128)(2,1)}), bf16[8,768,256]{1,2,0:T(8,128)(2,1)S(1)}, u32[]{:S(2)}, u32[]{:S(2)}) async-start(bf16[8,768,256]{1,2,0:T(8,128)(2,1)} %broadcast_in_dim.16), calls=%async_computation.4 | async-start | bytes 6291456 | tf_op jit(solution)/shard_map/all_to_all | solution.py:34
  216.1 195.6 %all-to-all-start.3 = ((bf16[16,128,2048]{2,1,0:T(8,128)(2,1)}), bf16[16,128,2048]{2,1,0:T(8,128)(2,1)}, u32[]{:S(2)}, u32[]{:S(2)}) async-start(bf16[16,128,2048]{2,1,0:T(8,128)(2,1)} %stack.2), calls=%async_computation.3 | async-start | bytes 16777216 | tf_op jit(solution)/shard_map/all_to_all | solution.py:15
  228.7 0.7 copy-start.11
  422.8 42.9 %copy-start.1 = (bf16[1,256,256]{2,1,0:T(8,128)(2,1)S(1)}, bf16[1,256,256]{2,1,0:T(8,128)(2,1)}, u32[]{:S(2)}) copy-start(bf16[1,256,256]{2,1,0:T(8,128)(2,1)} %param.17) | copy-start | bytes 393220
  463.8 1.0 copy-start.3
Sparse Core Ops, SparseCore 0:
  9.1 80.5 all-gather.1
